TPU v7x, 32 devices: a whole 2x2x4 slice. The times are simulated.
32 devices in a mesh: ep: 8 (over z, core), tp: 4 (over y, x).
Axes of the slice: x: 2, y: 2, z: 4, core: 2. Of those that a mesh axis runs over, the one named last changes fastest.
Arguments:
- tokens: bfloat16 [128, 2048], P('ep'), may hold values from -6 to 6
- norm_gain: float32 [2048], replicated, may hold values from 0.1 to 1.9
- w_query: bfloat16 [2048, 512], P('ep', 'tp'), may hold values from -0.125 to 0.125
- w_key: bfloat16 [2048, 512], P('ep', 'tp'), may hold values from -0.125 to 0.125
- w_decay: bfloat16 [2048, 512], P('ep', 'tp'), may hold values from -0.125 to 0.125
- w_value: bfloat16 [2048, 1024], P('ep', 'tp'), may hold values from -0.125 to 0.125
- w_outgate: bfloat16 [2048, 1024], P('ep', 'tp'), may hold values from -0.125 to 0.125
- decay_rate: float32 [512], P('tp'), may hold values from 0.02 to 1
- state: float32 [128, 4, 128, 256], P('ep', 'tp'), may hold values from -15 to 15
- head_gain: float32 [256], replicated, may hold values from 0.1 to 1.9
- w_output: bfloat16 [1024, 2048], P('tp'), may hold values from -0.1875 to 0.1875
- moe_gain: float32 [2048], replicated, may hold values from 0.1 to 1.9
- expert_ids: int32 [128, 2], P('ep'), may hold values from 0 to 7, all different within a row; in each aligned block of 16 rows (0 to 15, 16 to 31, ...) at most 8 rows name the same one
- group_prob: float32 [128], P('ep'), may hold values from 0.3 to 1
- inner_prob: float32 [128, 2], P('ep'), may hold values from 0.05 to 1
- w_gate: bfloat16 [8, 2048, 2048], P('ep', None, 'tp'), may hold values from -0.125 to 0.125
- w_up: bfloat16 [8, 2048, 2048], P('ep', None, 'tp'), may hold values from -0.125 to 0.125
- w_down: bfloat16 [8, 2048, 2048], P('ep', 'tp'), may hold values from -0.125 to 0.125
Outputs:
- output: bfloat16 [128, 2048], P('ep', 'tp')
Inputs may be any that keep to these rules, and one draw needn't show every extreme that they name: `expert_ids`: the 2 experts of a token differ. In the rows of one index of ep no expert is named more than 8 times, a bound that some block reaches there.
All inputs are finite; a program needn't handle non-finite values.
Results may differ from a plain program's by a relative error of at most 0.025.
Values may be sent and summed in bfloat16 or wider, within the bound.
A program may use at most 64 MiB of HBM per device.

v0:
```python
import jax
import jax.numpy as jnp
from jax import lax
from jax.sharding import PartitionSpec as P

epsilon = 1e-05


def inverse_rms(values):
    return lax.rsqrt(jnp.mean(values * values, axis=-1, keepdims=True) + epsilon)


def slot_numbers(route_ids, experts, capacity):
    flat_ids = route_ids.reshape(-1)
    onehot = (flat_ids[:, None] == jnp.arange(experts, dtype=jnp.int32)[None, :]).astype(jnp.int32)
    earlier = jnp.cumsum(onehot, axis=0) - onehot
    within = jnp.sum(earlier * onehot, axis=1)
    return (flat_ids * capacity + within).reshape(route_ids.shape)


def expert_apply(rows, weight_gate, weight_up, weight_down):
    gate = jnp.dot(rows, weight_gate, preferred_element_type=jnp.float32)
    upper = jnp.dot(rows, weight_up, preferred_element_type=jnp.float32)
    hidden = (jax.nn.silu(gate) * upper).astype(jnp.bfloat16)
    block_out = jnp.dot(hidden, weight_down, preferred_element_type=jnp.float32).astype(
        jnp.bfloat16
    )
    summed = lax.psum_scatter(
        block_out.astype(jnp.float32).astype(jnp.bfloat16), "tp", scatter_dimension=1, tiled=True
    )
    return summed


def on_device(
    tokens,
    norm_gain,
    w_query,
    w_key,
    w_decay,
    w_value,
    w_outgate,
    decay_rate,
    state,
    head_gain,
    w_output,
    moe_gain,
    expert_ids,
    group_prob,
    inner_prob,
    w_gate,
    w_up,
    w_down,
):
    wide = jnp.float32
    narrow = jnp.bfloat16
    seq_count = tokens.shape[0]
    model_width = tokens.shape[1]
    ep_count = lax.axis_size("ep")
    heads = state.shape[1]
    key_width = state.shape[2]
    value_width = state.shape[3]
    residual = tokens.astype(wide)
    normed = (residual * inverse_rms(residual) * norm_gain).astype(narrow)
    weights = (w_query, w_key, w_decay, w_value, w_outgate)
    spread = lax.all_to_all(normed, "ep", split_axis=1, concat_axis=0, tiled=True)
    projected = lax.psum_scatter(
        jnp.concatenate(
            [jnp.dot(spread, weight, preferred_element_type=wide) for weight in weights], axis=1
        ).astype(jnp.bfloat16),
        "ep",
        scatter_dimension=0,
        tiled=True,
    ).astype(jnp.float32)
    query_cols = w_query.shape[1]
    value_cols = w_value.shape[1]
    query = projected[:, :query_cols].astype(narrow).astype(wide).reshape(
        seq_count, heads, key_width
    ) * key_width ** (-0.5)
    key_rows = (
        projected[:, query_cols : 2 * query_cols]
        .astype(narrow)
        .astype(wide)
        .reshape(seq_count, heads, key_width)
    )
    decay_pre = projected[:, 2 * query_cols : 3 * query_cols]
    value_rows = (
        projected[:, 3 * query_cols : 3 * query_cols + value_cols].astype(narrow).astype(wide)
    )
    value_rows = value_rows.reshape(seq_count, heads, value_width)
    gate_rows = (
        projected[:, 3 * query_cols + value_cols :]
        .astype(narrow)
        .astype(wide)
        .reshape(seq_count, heads, value_width)
    )
    decay = jnp.exp(jax.nn.log_sigmoid(decay_pre) * decay_rate).reshape(seq_count, heads, key_width)
    updated = decay[..., None] * state + key_rows[..., None] * value_rows[:, :, None, :]
    readout = jnp.einsum("shk,shkv->shv", query, updated, precision=lax.Precision.HIGHEST)
    gated = (readout * inverse_rms(readout) * head_gain * jax.nn.silu(gate_rows)).astype(narrow)
    head_part = jnp.dot(
        gated.reshape(seq_count, heads * value_width), w_output, preferred_element_type=wide
    )
    attention = lax.psum(head_part.astype(narrow).astype(wide).astype(jnp.bfloat16), "tp").astype(
        jnp.float32
    )
    mixed_wide = (residual + attention).astype(narrow).astype(wide)
    moe_in = (mixed_wide * inverse_rms(mixed_wide) * moe_gain).astype(narrow)
    route_weight = group_prob[:, None] * inner_prob / jnp.sum(inner_prob, axis=1, keepdims=True)
    top = expert_ids.shape[1]
    capacity = 2 * seq_count * top // ep_count
    slot_total = ep_count * capacity
    col_width = model_width // lax.axis_size("tp")
    col_start = lax.axis_index("tp") * col_width
    slots = slot_numbers(expert_ids, ep_count, capacity)
    slot_range = jnp.arange(slot_total, dtype=jnp.int32)
    combine = jnp.sum(
        jnp.where(slots[:, :, None] == slot_range[None, None, :], route_weight[:, :, None], 0.0),
        axis=1,
    )
    dispatch = jnp.any(slots[None, :, :] == slot_range[:, None, None], axis=2).astype(narrow)
    sending = jnp.dot(dispatch, moe_in, preferred_element_type=wide).astype(narrow)
    arrived = lax.all_to_all(sending, "ep", split_axis=0, concat_axis=0, tiled=True)
    expert_out = expert_apply(arrived, w_gate[0], w_up[0], w_down[0])
    returned = lax.all_to_all(expert_out, "ep", split_axis=0, concat_axis=0, tiled=True).astype(
        wide
    )
    moe_sum = jnp.dot(combine, returned, precision=lax.Precision.HIGHEST)
    own_cols = lax.dynamic_slice_in_dim(mixed_wide, col_start, col_width, 1)
    return (own_cols + moe_sum).astype(narrow)


def solution(mesh):
    placed = (
        P("ep", None),
        P(),
        P("ep", "tp"),
        P("ep", "tp"),
        P("ep", "tp"),
        P("ep", "tp"),
        P("ep", "tp"),
        P("tp"),
        P("ep", "tp", None, None),
        P(),
        P("tp", None),
        P(),
        P("ep", None),
        P("ep"),
        P("ep", None),
        P("ep", None, "tp"),
        P("ep", None, "tp"),
        P("ep", "tp", None),
    )
    return jax.shard_map(
        on_device, mesh=mesh, in_specs=placed, out_specs=P("ep", "tp"), check_vma=False
    )
```

profile of v0, /device:TPU:0, one launch (start us, length us, event | category | flops | bytes accessed | tf_op | source)
XLA Modules:
  0.0 166.4 jit_solution(632470645362486646)
XLA Ops:
  6.5 1.1 fusion.28
  7.7 0.9 fusion.30
  8.6 0.0 copy-start.7
  8.6 0.6 copy.56
  9.2 6.4 %all-to-all-start = ((bf16[16,8,256]{2,0,1:T(8,128)(2,1)}), bf16[16,8,256]{2,0,1:T(8,128)(2,1)S(1)}, u32[]{:S(2)}, u32[]{:S(2)}) async-start(bf16[16,8,256]{2,0,1:T(8,128)(2,1)} %bitcast.65), calls=%async_computation | async-start | bytes 131072 | tf_op jit(solution)/shard_map/all_to_all | solution.py:65
  15.6 0.0 reduce-scatter.3.cloned.1.call-start
  15.6 0.8 copy.47
  16.4 0.1 eq.20
  16.5 5.0 %all-to-all-done = bf16[16,8,256]{2,0,1:T(8,128)(2,1)S(1)} async-done(((bf16[16,8,256]{2,0,1:T(8,128)(2,1)}), bf16[16,8,256]{2,0,1:T(8,128)(2,1)S(1)}, u32[]{:S(2)}, u32[]{:S(2)}) %all-to-all-start) | async-done | bytes 65568 | tf_op jit(solution)/shard_map/all_to_all | solution.py:65
  21.5 1.1 convolution_convert_fusion.7
  22.6 0.1 copy.44
  22.7 1.1 convolution_convert_fusion.6
  23.8 0.1 copy.45
  23.9 1.1 convolution_convert_fusion.5
  25.0 0.1 copy.46
  25.1 1.1 fusion.18
  26.2 0.0 copy-start.4
  26.2 1.1 fusion.17
  27.3 0.7 copy-done.3
  28.0 0.0 reduce-scatter.3.cloned.1.call-update
  28.0 0.0 all-reduce.2.cloned.1.call-start
  28.1 0.1 fusion.48
  28.1 0.1 reduce_window_sum.11
  28.2 0.2 select_reduce_fusion.1
  28.4 0.1 reduce_sum.59
  28.5 0.1 copy.48
  28.6 28.9 %reduce-scatter.3.cloned.1.call-done = bf16[16,896]{1,0:T(8,128)(2,1)} async-done(((bf16[128,896]{1,0:T(8,128)(2,1)}), bf16[16,896]{1,0:T(8,128)(2,1)}) %reduce-scatter.3.cloned.1.call-update) | async-done | bytes 28688 | tf_op jit(solution)/shard_map/reduce_scatter | solution.py:66
  57.4 0.7 slice_convert_fusion
  58.1 0.7 slice_convert_fusion.1
  58.8 0.7 fusion.54
  59.5 3.0 %fusion.6 = f32[16,1,256]{2,1,0:T(1,128)S(1)} fusion(f32[16,128,1]{1,2,0:T(1,128)S(1)} %bitcast.73, f32[16,1,128,256]{3,2,1,0:T(8,128)} %param.26, f32[16,256]{1,0:T(8,128)S(1)} %slice_convert_fusion, f32[16,128]{1,0:T(8,128)S(1)} %slice_convert_fusion.1, f32[16,128]{1,0:T(8,128)S(1)} %get-tuple-element.7), kind=kOutput, calls=%fused_computation.9 | convolution fusion | flops 7864320 | bytes 2154496 | tf_op jit(solution)/shard_map/shk,shkv->shv/dot_general | solution.py:98
  62.6 0.1 fusion.46
  62.7 1.6 convolution_convert_fusion.2
  64.3 0.0 all-reduce.2.cloned.1.call-update
  64.4 0.0 reduce-scatter.5.cloned.1.call-start
  64.4 0.1 fusion.50
  64.5 40.1 %all-reduce.2.cloned.1.call-done = bf16[16,2048]{1,0:T(8,128)(2,1)} async-done(((bf16[16,2048]{1,0:T(8,128)(2,1)}), bf16[16,2048]{1,0:T(8,128)(2,1)}) %all-reduce.2.cloned.1.call-update) | async-done | bytes 65552 | tf_op jit(solution)/shard_map/psum | solution.py:103
  104.6 1.0 fusion.37
  105.6 1.1 fusion
  106.7 14.1 %all_to_all.43 = bf16[8,8,2048]{2,1,0:T(8,128)(2,1)S(1)} all-to-all(bf16[8,8,2048]{2,1,0:T(8,128)(2,1)S(1)} %fusion), channel_id=1, replica_groups=mesh['ep'=8,'tp'=4] {'ep'}, dimensions={0} | all-to-all | bytes 524288 | tf_op jit(solution)/shard_map/all_to_all | solution.py:122
  120.8 2.1 %fusion.4 = f32[64,512]{1,0:T(8,128)S(1)} fusion(bf16[1,2048,512]{2,1,0:T(8,128)(2,1)} %param.33, bf16[8,8,2048]{2,1,0:T(8,128)(2,1)S(1)} %all_to_all.43), kind=kOutput, calls=%fused_computation.7 | convolution fusion | flops 134217728 | bytes 2490368 | tf_op jit(solution)/shard_map/dot_general | solution.py:22
  122.9 3.2 %convolution_convert_fusion = bf16[64,2048]{1,0:T(8,128)(2,1)} fusion(bf16[1,512,2048]{2,1,0:T(8,128)(2,1)S(1)} %copy-done, bf16[1,2048,512]{2,1,0:T(8,128)(2,1)} %param.34, bf16[8,8,2048]{2,1,0:T(8,128)(2,1)S(1)} %all_to_all.43, f32[64,512]{1,0:T(8,128)S(1)} %fusion.4), kind=kOutput, calls=%fused_computation | convolution fusion | flops 268763136 | bytes 4849664 | tf_op jit(solution)/shard_map/dot_general | solution.py:25
  126.1 0.0 reduce-scatter.5.cloned.1.call-update
  126.2 22.4 %reduce-scatter.5.cloned.1.call-done = bf16[64,512]{1,0:T(8,128)(2,1)} async-done(((bf16[64,2048]{1,0:T(8,128)(2,1)}), bf16[64,512]{1,0:T(8,128)(2,1)}) %reduce-scatter.5.cloned.1.call-update) | async-done | bytes 65552 | tf_op jit(solution)/shard_map/reduce_scatter | solution.py:28
  148.6 4.6 %all-to-all-start.2 = ((bf16[8,8,512]{2,1,0:T(8,128)(2,1)}), bf16[8,8,512]{2,1,0:T(8,128)(2,1)S(1)}, u32[]{:S(2)}, u32[]{:S(2)}) async-start(bf16[8,8,512]{2,1,0:T(8,128)(2,1)} %bitcast.72), calls=%async_computation.4 | async-start | bytes 131072 | tf_op jit(solution)/shard_map/all_to_all | solution.py:124
  153.2 0.1 select_reduce_fusion
  153.2 5.8 %all-to-all-done.2 = bf16[8,8,512]{2,1,0:T(8,128)(2,1)S(1)} async-done(((bf16[8,8,512]{2,1,0:T(8,128)(2,1)}), bf16[8,8,512]{2,1,0:T(8,128)(2,1)S(1)}, u32[]{:S(2)}, u32[]{:S(2)}) %all-to-all-start.2) | async-done | bytes 65568 | tf_op jit(solution)/shard_map/all_to_all | solution.py:124
  159.1 0.8 fusion.21
  (26 shorter events, 0.1 us)
Async XLA Ops:
  6.5 116.3 %copy-start = (bf16[1,512,2048]{2,1,0:T(8,128)(2,1)S(1)}, bf16[1,512,2048]{2,1,0:T(8,128)(2,1)}, u32[]{:S(2)}) copy-start(bf16[1,512,2048]{2,1,0:T(8,128)(2,1)} %param.35) | copy-start | bytes 6291460
  6.5 22.0 %copy-start.5 = (s32[16,2]{0,1:T(2,128)S(1)}, s32[16,2]{0,1:T(2,128)}, u32[]{:S(2)}) copy-start(s32[16,2]{0,1:T(2,128)} %param.30) | copy-start | bytes 388
  6.5 52.3 %copy-start.8 = (f32[128]{0:T(128)S(1)}, f32[128]{0:T(128)}, u32[]{:S(2)}) copy-start(f32[128]{0:T(128)} %param.25) | copy-start | bytes 1540
  8.6 54.1 %copy-start.1 = (bf16[256,2048]{1,0:T(8,128)(2,1)S(1)}, bf16[256,2048]{1,0:T(8,128)(2,1)}, u32[]{:S(2)}) copy-start(bf16[256,2048]{1,0:T(8,128)(2,1)} %param.28) | copy-start | bytes 3145732
  8.6 54.1 %copy-start.7 = (f32[256]{0:T(256)S(1)}, f32[256]{0:T(256)}, u32[]{:S(2)}) copy-start(f32[256]{0:T(256)} %param.27) | copy-start | bytes 3076
  9.2 12.3 %all-to-all-start = ((bf16[16,8,256]{2,0,1:T(8,128)(2,1)}), bf16[16,8,256]{2,0,1:T(8,128)(2,1)S(1)}, u32[]{:S(2)}, u32[]{:S(2)}) async-start(bf16[16,8,256]{2,0,1:T(8,128)(2,1)} %bitcast.65), calls=%async_computation | async-start | bytes 131072 | tf_op jit(solution)/shard_map/all_to_all | solution.py:65
  15.6 41.8 %reduce-scatter.3.cloned.1.call-start = ((), (), s32[]{:S(2)}) async-start(), calls=%async_computation.5 | async-start | bytes 258048 | tf_op jit(solution)/shard_map/reduce_scatter | solution.py:66
  25.1 79.4 %copy-start.2 = (bf16[16,2048]{1,0:T(8,128)(2,1)S(1)}, bf16[16,2048]{1,0:T(8,128)(2,1)}, u32[]{:S(2)}) copy-start(bf16[16,2048]{1,0:T(8,128)(2,1)} %param.18) | copy-start | bytes 196612
  26.2 79.3 %copy-start.4 = (f32[2048]{0:T(1024)S(1)}, f32[2048]{0:T(1024)}, u32[]{:S(2)}) copy-start(f32[2048]{0:T(1024)} %param.29) | copy-start | bytes 24580
  27.3 0.7 copy-start.3
  28.0 76.5 %all-reduce.2.cloned.1.call-start = ((), (), s32[]{:S(2)}) async-start(), calls=%async_computation.6 | async-start | bytes 131072 | tf_op jit(solution)/shard_map/psum | solution.py:103
  64.4 84.2 %reduce-scatter.5.cloned.1.call-start = ((), (), s32[]{:S(2)}) async-start(), calls=%async_computation.7 | async-start | bytes 327680 | tf_op jit(solution)/shard_map/reduce_scatter | solution.py:28
  122.9 3.3 %copy-start.6 = (f32[16,2]{0,1:T(2,128)S(1)}, f32[16,2]{0,1:T(2,128)}, u32[]{:S(2)}) copy-start(f32[16,2]{0,1:T(2,128)} %param.32) | copy-start | bytes 388
  122.9 3.3 %copy-start.9 = (f32[16]{0:T(128)S(1)}, f32[16]{0:T(128)}, u32[]{:S(2)}) copy-start(f32[16]{0:T(128)} %param.31) | copy-start | bytes 196
  148.6 10.5 %all-to-all-start.2 = ((bf16[8,8,512]{2,1,0:T(8,128)(2,1)}), bf16[8,8,512]{2,1,0:T(8,128)(2,1)S(1)}, u32[]{:S(2)}, u32[]{:S(2)}) async-start(bf16[8,8,512]{2,1,0:T(8,128)(2,1)} %bitcast.72), calls=%async_computation.4 | async-start | bytes 131072 | tf_op jit(solution)/shard_map/all_to_all | solution.py:124
Sparse Core Ops, SparseCore 0:
  28.1 29.2 reduce-scatter.2
  64.5 40.0 all-reduce.1
  126.2 22.2 reduce-scatter.4
where the time goes:
time: 167 us; the launch traced here: 166 us
  waiting for transfers between devices  102 us (61%)
  matrix products  17.1 us (10%)
  blocking collectives  14.1 us (8%)
  between operations  13.3 us (8%)
  starting transfers between devices  11.1 us (7%)
  other arithmetic  5.74 us (3%)
  local copies, waits for them, and re-layouts  2.73 us (2%)
    psum x1, waiting for transfers between devices, on_device(): lax.psum(head_part.astype(narrow).astype(wide).astype(jnp.bfloat16), 'tp')  40.1 us
    reduce_scatter x1, waiting for transfers between devices, on_device(): lax.psum_scatter(jnp.concatenate([jnp.dot(spread, weight, preferred_eleme...  28.9 us
    reduce_scatter x1, waiting for transfers between devices, expert_apply(): lax.psum_scatter(block_out.astype(jnp.float32).astype(jnp.bfloat16), 'tp'...  22.4 us
    all_to_all x1, blocking collectives, on_device(): lax.all_to_all(sending, 'ep', split_axis=0, concat_axis=0, tiled=True)  14.1 us
    all_to_all x1, starting transfers between devices, on_device(): lax.all_to_all(normed, 'ep', split_axis=1, concat_axis=0, tiled=True)  6.35 us
    all_to_all x1, waiting for transfers between devices, on_device(): lax.all_to_all(expert_out, 'ep', split_axis=0, concat_axis=0, tiled=True)  5.84 us
    dot_general x5, matrix products, on_device(): jnp.dot(spread, weight, preferred_element_type=wide)  5.33 us
    all_to_all x1, waiting for transfers between devices, on_device(): lax.all_to_all(normed, 'ep', split_axis=1, concat_axis=0, tiled=True)  5.03 us
  transfers between devices with their start and end apart: 5, of which 5 were waited for; matrix products, arithmetic and copies ran while one was open for 1% of the time, Pallas kernels for 0%

commit v1 on v0

--- a/solution.py
+++ b/solution.py
@@ -100,9 +100,9 @@
     head_part = jnp.dot(
         gated.reshape(seq_count, heads * value_width), w_output, preferred_element_type=wide
     )
-    attention = lax.psum(head_part.astype(narrow).astype(wide).astype(jnp.bfloat16), "tp").astype(
-        jnp.float32
-    )
+    attention = jnp.sum(
+        lax.all_gather(head_part.astype(narrow).astype(wide).astype(jnp.bfloat16), "tp"), axis=0
+    ).astype(jnp.float32)
     mixed_wide = (residual + attention).astype(narrow).astype(wide)
     moe_in = (mixed_wide * inverse_rms(mixed_wide) * moe_gain).astype(narrow)
     route_weight = group_prob[:, None] * inner_prob / jnp.sum(inner_prob, axis=1, keepdims=True)

time: 167 us -> 132 us (0.79)
  waiting for transfers between devices: 102 us -> 62.1 us
  blocking collectives: 14.1 us -> 21.1 us
    psum x1 -> x0, waiting for transfers between devices: 40.1 us -> none  [on_device(): lax.psum(head_part.astype(narrow).astype(wide).astype(jnp.bfloat16), 'tp')]
    all_gather x0 -> x1, blocking collectives: none -> 8.96 us  [on_device(): lax.all_gather(head_part.astype(narrow).astype(wide).astype(jnp.bfloat16)...]
    all_to_all x1, blocking collectives: 14.1 us -> 12.1 us  [on_device(): lax.all_to_all(sending, 'ep', split_axis=0, concat_axis=0, tiled=True)]
  transfers between devices with their start and end apart: 5 -> 4, of which waited for: 5 -> 4; matrix products, arithmetic and copies ran while one was open for 1% -> 1% of each run, Pallas kernels for 0% -> 0%
where the time goes in v1:
time: 132 us; the launch traced here: 131 us
  waiting for transfers between devices  62.1 us (47%)
  blocking collectives  21.1 us (16%)
  matrix products  15.6 us (12%)
  between operations  13.7 us (10%)
  starting transfers between devices  11 us (8%)
  other arithmetic  4.96 us (4%)
  local copies, waits for them, and re-layouts  2.73 us (2%)
    reduce_scatter x1, waiting for transfers between devices, on_device(): lax.psum_scatter(jnp.concatenate([jnp.dot(spread, weight, preferred_eleme...  28.8 us
    reduce_scatter x1, waiting for transfers between devices, expert_apply(): lax.psum_scatter(block_out.astype(jnp.float32).astype(jnp.bfloat16), 'tp'...  22.4 us
    all_to_all x1, blocking collectives, on_device(): lax.all_to_all(sending, 'ep', split_axis=0, concat_axis=0, tiled=True)  12.1 us
    all_gather x1, blocking collectives, on_device(): lax.all_gather(head_part.astype(narrow).astype(wide).astype(jnp.bfloat16)...  8.96 us
    all_to_all x1, starting transfers between devices, on_device(): lax.all_to_all(normed, 'ep', split_axis=1, concat_axis=0, tiled=True)  6.35 us
    all_to_all x1, waiting for transfers between devices, on_device(): lax.all_to_all(expert_out, 'ep', split_axis=0, concat_axis=0, tiled=True)  5.84 us
    dot_general x5, matrix products, on_device(): jnp.dot(spread, weight, preferred_element_type=wide)  5.3 us
    all_to_all x1, waiting for transfers between devices, on_device(): lax.all_to_all(normed, 'ep', split_axis=1, concat_axis=0, tiled=True)  5.03 us
  transfers between devices with their start and end apart: 4, of which 4 were waited for; matrix products, arithmetic and copies ran while one was open for 1% of the time, Pallas kernels for 0%

profile of v1, /device:TPU:0, one launch (start us, length us, event | category | flops | bytes accessed | tf_op | source)
XLA Modules:
  0.0 131.1 jit_solution(3891444344808829789)
XLA Ops:
  6.5 1.1 fusion.28
  7.7 0.9 fusion.30
  8.6 0.0 copy-start.1
  8.6 0.0 copy-start.7
  8.6 0.6 copy.56
  9.2 6.4 %all-to-all-start = ((bf16[16,8,256]{2,0,1:T(8,128)(2,1)}), bf16[16,8,256]{2,0,1:T(8,128)(2,1)S(1)}, u32[]{:S(2)}, u32[]{:S(2)}) async-start(bf16[16,8,256]{2,0,1:T(8,128)(2,1)} %bitcast.66), calls=%async_computation | async-start | bytes 131072 | tf_op jit(solution)/shard_map/all_to_all | solution.py:65
  15.6 0.0 reduce-scatter.3.cloned.1.call-start
  15.6 0.8 copy.47
  16.4 0.1 eq.20
  16.5 5.0 %all-to-all-done = bf16[16,8,256]{2,0,1:T(8,128)(2,1)S(1)} async-done(((bf16[16,8,256]{2,0,1:T(8,128)(2,1)}), bf16[16,8,256]{2,0,1:T(8,128)(2,1)S(1)}, u32[]{:S(2)}, u32[]{:S(2)}) %all-to-all-start) | async-done | bytes 65568 | tf_op jit(solution)/shard_map/all_to_all | solution.py:65
  21.5 1.1 convolution_convert_fusion.7
  22.6 0.1 copy.44
  22.7 1.1 convolution_convert_fusion.6
  23.8 0.1 copy.45
  23.9 1.1 convolution_convert_fusion.5
  25.0 0.1 copy.46
  25.1 1.1 fusion.18
  26.2 1.1 fusion.17
  27.3 0.7 copy-done.3
  27.9 0.0 reduce-scatter.3.cloned.1.call-update
  28.0 0.0 copy-start.2
  28.0 0.0 reduce-scatter.5.cloned.1.call-start
  28.0 0.1 fusion.48
  28.1 0.1 reduce_window_sum.11
  28.2 0.2 select_reduce_fusion.1
  28.3 0.1 reduce_sum.72
  28.4 0.1 copy.48
  28.5 0.1 fusion.50
  28.6 28.8 %reduce-scatter.3.cloned.1.call-done = bf16[16,896]{1,0:T(8,128)(2,1)} async-done(((bf16[128,896]{1,0:T(8,128)(2,1)}), bf16[16,896]{1,0:T(8,128)(2,1)}) %reduce-scatter.3.cloned.1.call-update) | async-done | bytes 28688 | tf_op jit(solution)/shard_map/reduce_scatter | solution.py:66
  57.4 0.7 slice_convert_fusion
  58.1 0.7 slice_convert_fusion.1
  58.8 0.7 fusion.54
  59.5 3.0 %fusion.6 = f32[16,1,256]{2,1,0:T(1,128)S(1)} fusion(f32[16,128,1]{1,2,0:T(1,128)S(1)} %bitcast.75, f32[16,1,128,256]{3,2,1,0:T(8,128)} %param.26, f32[16,256]{1,0:T(8,128)S(1)} %slice_convert_fusion, f32[16,128]{1,0:T(8,128)S(1)} %slice_convert_fusion.1, f32[16,128]{1,0:T(8,128)S(1)} %get-tuple-element.7), kind=kOutput, calls=%fused_computation.9 | convolution fusion | flops 7864320 | bytes 2154496 | tf_op jit(solution)/shard_map/shk,shkv->shv/dot_general | solution.py:98
  62.5 0.1 fusion.46
  62.7 1.0 convolution_convert_fusion.2
  63.7 9.0 %all-gather = bf16[64,2048]{1,0:T(8,128)(2,1)S(1)} all-gather(bf16[16,2048]{1,0:T(8,128)(2,1)S(1)} %convolution_convert_fusion.2), channel_id=2, replica_groups=mesh['ep'=8,'tp'=4] {'tp'}, dimensions={0}, use_global_device_ids=true | all-gather | bytes 327680 | tf_op jit(solution)/shard_map/all_gather | solution.py:104
  72.7 0.1 fusion.37
  72.8 0.3 fusion
  73.1 12.1 %all_to_all.43 = bf16[8,8,2048]{2,1,0:T(8,128)(2,1)S(1)} all-to-all(bf16[8,8,2048]{2,1,0:T(8,128)(2,1)S(1)} %fusion), channel_id=1, replica_groups=mesh['ep'=8,'tp'=4] {'ep'}, dimensions={0} | all-to-all | bytes 524288 | tf_op jit(solution)/shard_map/all_to_all | solution.py:122
  85.2 2.1 %fusion.4 = f32[64,512]{1,0:T(8,128)S(1)} fusion(bf16[1,2048,512]{2,1,0:T(8,128)(2,1)} %param.33, bf16[8,8,2048]{2,1,0:T(8,128)(2,1)S(1)} %all_to_all.43), kind=kOutput, calls=%fused_computation.7 | convolution fusion | flops 134217728 | bytes 2490368 | tf_op jit(solution)/shard_map/dot_general | solution.py:22
  87.3 0.0 copy-start.9
  87.3 3.2 %convolution_convert_fusion = bf16[64,2048]{1,0:T(8,128)(2,1)} fusion(bf16[1,512,2048]{2,1,0:T(8,128)(2,1)S(1)} %copy-done, bf16[1,2048,512]{2,1,0:T(8,128)(2,1)} %param.34, bf16[8,8,2048]{2,1,0:T(8,128)(2,1)S(1)} %all_to_all.43, f32[64,512]{1,0:T(8,128)S(1)} %fusion.4), kind=kOutput, calls=%fused_computation | convolution fusion | flops 268763136 | bytes 4849664 | tf_op jit(solution)/shard_map/dot_general | solution.py:25
  90.5 0.0 reduce-scatter.5.cloned.1.call-update
  90.6 22.4 %reduce-scatter.5.cloned.1.call-done = bf16[64,512]{1,0:T(8,128)(2,1)} async-done(((bf16[64,2048]{1,0:T(8,128)(2,1)}), bf16[64,512]{1,0:T(8,128)(2,1)}) %reduce-scatter.5.cloned.1.call-update) | async-done | bytes 65552 | tf_op jit(solution)/shard_map/reduce_scatter | solution.py:28
  113.0 4.6 %all-to-all-start.2 = ((bf16[8,8,512]{2,1,0:T(8,128)(2,1)}), bf16[8,8,512]{2,1,0:T(8,128)(2,1)S(1)}, u32[]{:S(2)}, u32[]{:S(2)}) async-start(bf16[8,8,512]{2,1,0:T(8,128)(2,1)} %bitcast.74), calls=%async_computation.4 | async-start | bytes 131072 | tf_op jit(solution)/shard_map/all_to_all | solution.py:124
  117.6 0.1 select_reduce_fusion
  117.7 5.8 %all-to-all-done.2 = bf16[8,8,512]{2,1,0:T(8,128)(2,1)S(1)} async-done(((bf16[8,8,512]{2,1,0:T(8,128)(2,1)}), bf16[8,8,512]{2,1,0:T(8,128)(2,1)S(1)}, u32[]{:S(2)}, u32[]{:S(2)}) %all-to-all-start.2) | async-done | bytes 65568 | tf_op jit(solution)/shard_map/all_to_all | solution.py:124
  123.5 0.8 fusion.21
  (25 shorter events, 0.2 us)
Async XLA Ops:
  6.5 80.8 %copy-start = (bf16[1,512,2048]{2,1,0:T(8,128)(2,1)S(1)}, bf16[1,512,2048]{2,1,0:T(8,128)(2,1)}, u32[]{:S(2)}) copy-start(bf16[1,512,2048]{2,1,0:T(8,128)(2,1)} %param.35) | copy-start | bytes 6291460
  6.5 22.0 %copy-start.5 = (s32[16,2]{0,1:T(2,128)S(1)}, s32[16,2]{0,1:T(2,128)}, u32[]{:S(2)}) copy-start(s32[16,2]{0,1:T(2,128)} %param.30) | copy-start | bytes 388
  6.5 52.2 %copy-start.8 = (f32[128]{0:T(128)S(1)}, f32[128]{0:T(128)}, u32[]{:S(2)}) copy-start(f32[128]{0:T(128)} %param.25) | copy-start | bytes 1540
  8.6 54.1 %copy-start.1 = (bf16[256,2048]{1,0:T(8,128)(2,1)S(1)}, bf16[256,2048]{1,0:T(8,128)(2,1)}, u32[]{:S(2)}) copy-start(bf16[256,2048]{1,0:T(8,128)(2,1)} %param.28) | copy-start | bytes 3145732
  8.6 54.1 %copy-start.7 = (f32[256]{0:T(256)S(1)}, f32[256]{0:T(256)}, u32[]{:S(2)}) copy-start(f32[256]{0:T(256)} %param.27) | copy-start | bytes 3076
  9.2 12.3 %all-to-all-start = ((bf16[16,8,256]{2,0,1:T(8,128)(2,1)}), bf16[16,8,256]{2,0,1:T(8,128)(2,1)S(1)}, u32[]{:S(2)}, u32[]{:S(2)}) async-start(bf16[16,8,256]{2,0,1:T(8,128)(2,1)} %bitcast.66), calls=%async_computation | async-start | bytes 131072 | tf_op jit(solution)/shard_map/all_to_all | solution.py:65
  15.6 41.8 %reduce-scatter.3.cloned.1.call-start = ((), (), s32[]{:S(2)}) async-start(), calls=%async_computation.5 | async-start | bytes 258048 | tf_op jit(solution)/shard_map/reduce_scatter | solution.py:66
  27.3 0.7 copy-start.3
  28.0 44.7 %copy-start.2 = (bf16[16,2048]{1,0:T(8,128)(2,1)S(1)}, bf16[16,2048]{1,0:T(8,128)(2,1)}, u32[]{:S(2)}) copy-start(bf16[16,2048]{1,0:T(8,128)(2,1)} %param.18) | copy-start | bytes 196612
  28.0 85.0 %reduce-scatter.5.cloned.1.call-start = ((), (), s32[]{:S(2)}) async-start(), calls=%async_computation.6 | async-start | bytes 327680 | tf_op jit(solution)/shard_map/reduce_scatter | solution.py:28
  59.5 13.3 %copy-start.4 = (f32[2048]{0:T(1024)S(1)}, f32[2048]{0:T(1024)}, u32[]{:S(2)}) copy-start(f32[2048]{0:T(1024)} %param.29) | copy-start | bytes 24580
  87.3 3.3 %copy-start.6 = (f32[16,2]{0,1:T(2,128)S(1)}, f32[16,2]{0,1:T(2,128)}, u32[]{:S(2)}) copy-start(f32[16,2]{0,1:T(2,128)} %param.32) | copy-start | bytes 388
  87.3 3.3 %copy-start.9 = (f32[16]{0:T(128)S(1)}, f32[16]{0:T(128)}, u32[]{:S(2)}) copy-start(f32[16]{0:T(128)} %param.31) | copy-start | bytes 196
  113.0 10.5 %all-to-all-start.2 = ((bf16[8,8,512]{2,1,0:T(8,128)(2,1)}), bf16[8,8,512]{2,1,0:T(8,128)(2,1)S(1)}, u32[]{:S(2)}, u32[]{:S(2)}) async-start(bf16[8,8,512]{2,1,0:T(8,128)(2,1)} %bitcast.74), calls=%async_computation.4 | async-start | bytes 131072 | tf_op jit(solution)/shard_map/all_to_all | solution.py:124
Sparse Core Ops, SparseCore 0:
  28.1 29.2 reduce-scatter.2
  90.7 22.2 reduce-scatter.4
